TPU v7x, 32 devices: a whole 2x2x4 slice. The times are simulated.
32 devices in a mesh: fs: 8 (over z, y), tp: 4 (over x, core).
Axes of the slice: x: 2, y: 2, z: 4, core: 2. Of those that a mesh axis runs over, the one named last changes fastest.
Arguments:
- inputs: bfloat16 [4608, 2048], P('fs'), may hold values from -6 to 6
- query_cotangent: bfloat16 [4608, 1024], P('fs', 'tp'), may hold values from -0.017944336 to 0.017944336
- value_cotangent: bfloat16 [4608, 1024], P('fs', 'tp'), may hold values from -0.017944336 to 0.017944336
- weights_query: float32 [2048, 1024], P('fs', 'tp'), may hold values from -6 to 6
- weights_value: float32 [2048, 1024], P('fs', 'tp'), may hold values from -6 to 6
- basis_query: bfloat16 [1024, 32], P('tp'), may hold values from -0.75 to 0.75
- basis_value: bfloat16 [1024, 32], P('tp'), may hold values from -0.75 to 0.75
- first_query: float32 [2048, 512], P('fs', 'tp'), may hold values from -5.4 to 5.4, as said below
- second_query: float32 [2048, 512], P('fs', 'tp'), may hold values from 0.05 to 1
- first_value: float32 [2048, 512], P('fs', 'tp'), may hold values from -5.4 to 5.4, as said below
- second_value: float32 [2048, 512], P('fs', 'tp'), may hold values from 0.05 to 1
Outputs:
- step_query: float32 [2048, 1024], P('fs', 'tp')
- step_value: float32 [2048, 1024], P('fs', 'tp')
- new_query: float32 [2048, 1024], P('fs', 'tp')
- new_value: float32 [2048, 1024], P('fs', 'tp')
- copy_query: bfloat16 [2048, 1024], P(None, 'tp')
- copy_value: bfloat16 [2048, 1024], P(None, 'tp')
- moment_query: float32 [2048, 512], P('fs', 'tp')
- square_query: float32 [2048, 512], P('fs', 'tp')
- moment_value: float32 [2048, 512], P('fs', 'tp')
- square_value: float32 [2048, 512], P('fs', 'tp')
Inputs may be any that keep to these rules, and one draw needn't show every extreme that they name: `first_query`: first moments, with a spread of scale from row to row. `first_value`: first moments, with a spread of scale from row to row.
All inputs are finite; a program needn't handle non-finite values.
Results may differ from a plain program's by a relative error of at most 0.003.
Values may be sent and summed in bfloat16 or wider, within the bound.
A program may use at most 64 MiB of HBM per device.

v0:
```python
import jax
import jax.numpy as jnp
from jax import lax
from jax.sharding import PartitionSpec as P

D = 2048
HEADS = 16
HEAD = 64
RK = 32


def from_space(direction, factor, heads_here):
    count = direction.shape[0]
    split = direction.reshape(count, heads_here, RK)
    out = jnp.einsum("nhr,hdr->nhd", split, factor, precision=lax.Precision.HIGHEST)
    return out.reshape(count, heads_here * HEAD)


def moments(reduced, first, second):
    moment = 0.9 * first + 0.1 * reduced
    square = 0.95 * second + 0.05 * reduced * reduced
    direction = moment / (jnp.sqrt(square) + 1e-08)
    return (moment, square, direction)


def per_device(
    inputs,
    query_cotangent,
    value_cotangent,
    weights_query,
    weights_value,
    basis_query,
    basis_value,
    first_query,
    second_query,
    first_value,
    second_value,
):
    own_cols = weights_query.shape[1]
    heads_here = own_cols // HEAD
    space_cols = heads_here * RK
    factor_q = basis_query.reshape(heads_here, HEAD, RK).astype(jnp.float32)
    factor_v = basis_value.reshape(heads_here, HEAD, RK).astype(jnp.float32)
    contract = (((0,), (0,)), ((), ()))
    tok_count = query_cotangent.shape[0]
    bf_q = basis_query.reshape(heads_here, HEAD, RK)
    bf_v = basis_value.reshape(heads_here, HEAD, RK)
    small_q = jnp.einsum(
        "thd,hdr->thr",
        query_cotangent.reshape(tok_count, heads_here, HEAD),
        bf_q,
        preferred_element_type=jnp.float32,
    )
    small_v = jnp.einsum(
        "thd,hdr->thr",
        value_cotangent.reshape(tok_count, heads_here, HEAD),
        bf_v,
        preferred_element_type=jnp.float32,
    )
    small_both = jnp.concatenate(
        (small_q.reshape(tok_count, space_cols), small_v.reshape(tok_count, space_cols)), axis=1
    )
    upper_part = small_both.astype(jnp.bfloat16)
    lower_part = (small_both - upper_part.astype(jnp.float32)).astype(jnp.bfloat16)
    high = lax.dot_general(inputs, upper_part, contract, preferred_element_type=jnp.float32)
    reduced = lax.psum_scatter(
        high + lax.dot_general(inputs, lower_part, contract, preferred_element_type=jnp.float32),
        "fs",
        scatter_dimension=0,
        tiled=True,
    )
    reduced_q = reduced[:, :space_cols]
    reduced_v = reduced[:, space_cols:]
    moment_q, square_q, direction_q = moments(reduced_q, first_query, second_query)
    moment_v, square_v, direction_v = moments(reduced_v, first_value, second_value)
    total_q, total_v = lax.psum(
        (jnp.sum(direction_q * direction_q), jnp.sum(direction_v * direction_v)), ("fs", "tp")
    )
    entries = D * HEADS * RK
    scale_q = 1.0 / jnp.sqrt(total_q / entries + 0.25)
    scale_v = 1.0 / jnp.sqrt(total_v / entries + 0.25)
    step_q = scale_q * from_space(direction_q, factor_q, heads_here)
    step_v = scale_v * from_space(direction_v, factor_v, heads_here)
    fresh_q = weights_query - 0.1 * step_q
    fresh_v = weights_value - 0.1 * step_v
    copy_q, copy_v = (
        lax.all_gather(fresh_q.astype(jnp.bfloat16), "fs", axis=0, tiled=True),
        lax.all_gather(fresh_v.astype(jnp.bfloat16), "fs", axis=0, tiled=True),
    )
    return (
        step_q,
        step_v,
        fresh_q,
        fresh_v,
        copy_q,
        copy_v,
        moment_q,
        square_q,
        moment_v,
        square_v,
    )


def solution(mesh):
    placed = (
        P("fs", None),
        P("fs", "tp"),
        P("fs", "tp"),
        P("fs", "tp"),
        P("fs", "tp"),
        P("tp", None),
        P("tp", None),
        P("fs", "tp"),
        P("fs", "tp"),
        P("fs", "tp"),
        P("fs", "tp"),
    )
    return jax.shard_map(
        per_device,
        mesh=mesh,
        in_specs=placed,
        out_specs=(
            P("fs", "tp"),
            P("fs", "tp"),
            P("fs", "tp"),
            P("fs", "tp"),
            P(None, "tp"),
            P(None, "tp"),
            P("fs", "tp"),
            P("fs", "tp"),
            P("fs", "tp"),
            P("fs", "tp"),
        ),
        check_vma=False,
    )
```

profile of v0, /device:TPU:0, one launch (start us, length us, event | category | flops | bytes accessed | tf_op | source)
XLA Modules:
  0.0 223.8 jit_solution(16746739006652718097)
XLA Ops:
  7.2 0.0 copy-start
  7.2 0.0 reduce-scatter.2.cloned.1.call-start
  7.2 1.0 reshape.52
  8.2 0.0 copy-start.4
  8.2 0.8 reshape.55
  9.0 1.2 copy.40
  10.2 1.2 copy.42
  11.4 0.2 fusion.10
  11.6 0.2 fusion.7
  11.7 0.0 copy-done
  11.8 1.0 fusion.2
  12.8 0.0 copy-done.4
  12.8 0.0 copy-start.5
  12.8 2.3 %fusion = f32[2048,256]{0,1:T(8,128)} fusion(f32[256,2048]{1,0:T(8,128)S(1)} %fusion.2, bf16[576,2048]{1,0:T(8,128)(2,1)S(1)} %copy-done, f32[576,128]{0,1:T(8,128)S(1)} %bitcast.31, f32[576,128]{0,1:T(8,128)S(1)} %bitcast.29), kind=kOutput, calls=%fused_computation.1 | convolution fusion | flops 605241344 | bytes 7143424 | tf_op jit(solution)/shard_map/dot_general | solution.py:67
  15.1 0.0 reduce-scatter.2.cloned.1.call-update
  15.2 0.0 all-gather.5.cloned.1.call-start
  15.2 0.0 copy-done.5
  15.2 0.1 copy.39
  15.3 0.7 copy-done.6
  16.0 0.1 copy.44
  16.1 0.0 copy-done.7
  16.1 0.1 copy.46
  16.3 0.0 copy-done.8
  16.3 0.1 copy.47
  16.4 70.6 %reduce-scatter.2.cloned.1.call-done = f32[256,256]{0,1:T(8,128)} async-done(((f32[2048,256]{0,1:T(8,128)}), f32[256,256]{0,1:T(8,128)}) %reduce-scatter.2.cloned.1.call-update) | async-done | bytes 262160 | tf_op jit(solution)/shard_map/reduce_scatter | solution.py:66
  86.9 2.4 %multiply_reduce_fusion = (f32[]{:T(128)}, f32[256,128]{0,1:T(8,128)S(1)}, f32[256,128]{0,1:T(8,128)}, f32[256,128]{0,1:T(8,128)S(1)}, f32[]{:T(128)}, /*index=5...) fusion(f32[256,256]{0,1:T(8,128)} %reduce-scatter.2.cloned.1.call-done, f32[256,128]{0,1:T(8,128)S(1)} %copy.47, ...), kind=kLoop, calls=%fused_computation.14 | loop fusion | flops 720894 | bytes 1572872 | tf_op jit(solution)/shard_map/reduce_sum | solution.py:77
  89.3 39.8 %all-reduce = (f32[]{:T(128)}, f32[]{:T(128)}) all-reduce(f32[]{:T(128)} %get-tuple-element.44, f32[]{:T(128)} %get-tuple-element.36), channel_id=1, replica_groups=mesh['fs'=8,'tp'=4] {'fs','tp'}, use_global_device_ids=true, to_apply=%region_2.0 | all-reduce | flops 2 | bytes 16 | tf_op jit(solution)/shard_map/psum | solution.py:76
  129.8 0.3 convolution_multiply_fusion
  130.1 0.1 copy.52
  130.3 0.0 copy-start.1
  130.3 1.8 fusion.14
  132.1 0.0 all-gather.5.cloned.1.call-update
  132.1 0.0 all-gather.3.cloned.1.call-start
  132.9 1.2 convolution_multiply_fusion.1
  134.1 0.1 copy.51
  134.2 0.0 copy-start.2
  134.2 1.8 fusion.15
  136.1 0.0 all-gather.3.cloned.1.call-update
  136.1 1.7 copy.56
  137.8 0.8 copy.55
  138.5 0.8 copy.54
  139.3 0.8 copy.53
  140.0 32.2 %all-gather.5.cloned.1.call-done = bf16[2048,256]{1,0:T(8,128)(2,1)} async-done(((bf16[256,256]{1,0:T(8,128)(2,1)}), bf16[2048,256]{1,0:T(8,128)(2,1)}) %all-gather.5.cloned.1.call-update) | async-done | bytes 1048592 | tf_op jit(solution)/shard_map/all_gather | solution.py:88
  172.3 41.7 %all-gather.3.cloned.1.call-done = bf16[2048,256]{1,0:T(8,128)(2,1)} async-done(((bf16[256,256]{1,0:T(8,128)(2,1)}), bf16[2048,256]{1,0:T(8,128)(2,1)}) %all-gather.3.cloned.1.call-update) | async-done | bytes 1048592 | tf_op jit(solution)/shard_map/all_gather | solution.py:87
  214.0 2.4 %copy.67 = bf16[2048,256]{1,0:T(8,128)(2,1)} copy(bf16[2048,256]{1,0:T(8,128)(2,1)} %all-gather.3.cloned.1.call-done) | data formatting | bytes 2097152
  216.3 0.0 copy-done.1
  216.3 1.0 copy.68
  217.3 0.0 copy-done.2
  (5 shorter events, 0.0 us)
Async XLA Ops:
  7.2 4.6 %copy-start = (bf16[576,2048]{1,0:T(8,128)(2,1)S(1)}, bf16[576,2048]{1,0:T(8,128)(2,1)}, u32[]{:S(2)}) copy-start(bf16[576,2048]{1,0:T(8,128)(2,1)} %param.11) | copy-start | bytes 7077892
  7.2 79.7 %reduce-scatter.2.cloned.1.call-start = ((), (), s32[]{:S(2)}) async-start(), calls=%async_computation.1 | async-start | bytes 2359296 | tf_op jit(solution)/shard_map/reduce_scatter | solution.py:66
  8.2 4.6 %copy-start.4 = (bf16[4,64,32]{1,0,2:T(4,128)(2,1)}, bf16[4,64,32]{1,0,2:T(4,128)(2,1)S(1)}, u32[]{:S(2)}) copy-start(bf16[4,64,32]{1,0,2:T(4,128)(2,1)S(1)} %reshape.52) | copy-start | bytes 49156
  12.8 2.4 %copy-start.5 = (f32[256,128]{1,0:T(8,128)S(1)}, f32[256,128]{1,0:T(8,128)}, u32[]{:S(2)}) copy-start(f32[256,128]{1,0:T(8,128)} %param.18) | copy-start | bytes 393220
  15.1 0.9 copy-start.6
  15.1 1.0 copy-start.7
  15.1 1.1 copy-start.8
  15.2 157.1 %all-gather.5.cloned.1.call-start = ((), (), s32[]{:S(2)}) async-start(), calls=%async_computation.3 | async-start | bytes 1179648 | tf_op jit(solution)/shard_map/all_gather | solution.py:88
  130.3 86.1 %copy-start.1 = (f32[256,256]{1,0:T(8,128)}, f32[256,256]{1,0:T(8,128)S(1)}, u32[]{:S(2)}) copy-start(f32[256,256]{1,0:T(8,128)S(1)} %copy.52) | copy-start | bytes 786436
  132.1 81.8 %all-gather.3.cloned.1.call-start = ((), (), s32[]{:S(2)}) async-start(), calls=%async_computation.2 | async-start | bytes 1179648 | tf_op jit(solution)/shard_map/all_gather | solution.py:87
  134.2 83.1 %copy-start.2 = (f32[256,256]{1,0:T(8,128)}, f32[256,256]{1,0:T(8,128)S(1)}, u32[]{:S(2)}) copy-start(f32[256,256]{1,0:T(8,128)S(1)} %copy.51) | copy-start | bytes 786436
  214.0 2.4 %copy-start.3 = (bf16[2048,256]{1,0:T(8,128)(2,1)S(1)}, bf16[2048,256]{1,0:T(8,128)(2,1)}, u32[]{:S(2)}) copy-start(bf16[2048,256]{1,0:T(8,128)(2,1)} %all-gather.5.cloned.1.call-done) | copy-start | bytes 3145732
Sparse Core Ops, SparseCore 0:
  15.3 71.6 reduce-scatter.1
  132.3 39.9 all-gather.4
  175.0 38.9 all-gather.2
where the time goes:
time: 224 us
  waiting for transfers between devices  145 us (65%)
  blocking collectives  39.8 us (18%)
  between operations  15.3 us (7%)
  local copies, waits for them, and re-layouts  12.7 us (6%)
  other arithmetic  6.06 us (3%)
  matrix products  5.25 us (2%)
    reduce_scatter x1, waiting for transfers between devices, per_device(): lax.psum_scatter(high + lax.dot_general(inputs, lower_part, contract, pre...  70.6 us
    all_gather x1, waiting for transfers between devices, per_device(): lax.all_gather(fresh_q.astype(jnp.bfloat16), 'fs', axis=0, tiled=True)  41.7 us
    psum x1, blocking collectives, per_device(): lax.psum((jnp.sum(direction_q * direction_q), jnp.sum(direction_v * direc...  39.8 us
    all_gather x1, waiting for transfers between devices, per_device(): lax.all_gather(fresh_v.astype(jnp.bfloat16), 'fs', axis=0, tiled=True)  32.2 us
    unnamed x32, local copies, waits for them, and re-layouts  11 us
  transfers between devices with their start and end apart: 3, of which 3 were waited for; matrix products, arithmetic and copies ran while one was open for 3% of the time, Pallas kernels for 0%

commit v1 on v0

--- a/solution.py
+++ b/solution.py
@@ -7,6 +7,18 @@
 HEADS = 16
 HEAD = 64
 RK = 32
+
+
+def gather_around(value, axis, dim):
+    ways, here, step = (lax.axis_size(axis), lax.axis_index(axis), value.shape[dim])
+    lengths = [n * ways if d == dim else n for d, n in enumerate(value.shape)]
+    full = lax.dynamic_update_slice_in_dim(
+        jnp.zeros(lengths, value.dtype), value, here * step, axis=dim
+    )
+    for far in range(1, ways):
+        value = lax.ppermute(value, axis, [(d, (d + 1) % ways) for d in range(ways)])
+        full = lax.dynamic_update_slice_in_dim(full, value, (here - far) % ways * step, axis=dim)
+    return full
 
 
 def from_space(direction, factor, heads_here):
@@ -84,7 +96,7 @@
     fresh_q = weights_query - 0.1 * step_q
     fresh_v = weights_value - 0.1 * step_v
     copy_q, copy_v = (
-        lax.all_gather(fresh_q.astype(jnp.bfloat16), "fs", axis=0, tiled=True),
+        gather_around(fresh_q.astype(jnp.bfloat16), "fs", 0),
         lax.all_gather(fresh_v.astype(jnp.bfloat16), "fs", axis=0, tiled=True),
     )
     return (

time: 224 us -> 205 us (0.915)
  waiting for transfers between devices: 145 us -> 114 us
  local copies, waits for them, and re-layouts: 12.7 us -> 19.8 us
  starting transfers between devices: 0.12 us -> 3.72 us
    ppermute x0 -> x7, waiting for transfers between devices: none -> 43.1 us  [gather_around(): lax.ppermute(value, axis, [(d, (d + 1) % ways) for d in range(ways)])]
    all_gather x1 -> x0, waiting for transfers between devices: 41.7 us -> none  [per_device(): lax.all_gather(fresh_q.astype(jnp.bfloat16), 'fs', axis=0, tiled=True)]
    all_gather x1, waiting for transfers between devices: 32.2 us -> 0.01 us  [per_device(): lax.all_gather(fresh_v.astype(jnp.bfloat16), 'fs', axis=0, tiled=True)]
    dynamic_update_slice x0 -> x7, local copies, waits for them, and re-layouts: none -> 7.36 us  [gather_around(): lax.dynamic_update_slice_in_dim(full, value, (here - far) % ways * step,...]
    ppermute x0 -> x7, starting transfers between devices: none -> 3.64 us  [gather_around(): lax.ppermute(value, axis, [(d, (d + 1) % ways) for d in range(ways)])]
    unnamed x32 -> x35, local copies, waits for them, and re-layouts: 11 us -> 9.67 us
  transfers between devices with their start and end apart: 3 -> 9, of which waited for: 3 -> 8; matrix products, arithmetic and copies ran while one was open for 3% -> 7% of each run, Pallas kernels for 0% -> 0%
where the time goes in v1:
time: 205 us
  waiting for transfers between devices  114 us (56%)
  blocking collectives  39.8 us (19%)
  local copies, waits for them, and re-layouts  19.8 us (10%)
  between operations  15.6 us (8%)
  other arithmetic  5.93 us (3%)
  matrix products  5.84 us (3%)
  starting transfers between devices  3.72 us (2%)
    reduce_scatter x1, waiting for transfers between devices, per_device(): lax.psum_scatter(high + lax.dot_general(inputs, lower_part, contract, pre...  70.9 us
    ppermute x7, waiting for transfers between devices, gather_around(): lax.ppermute(value, axis, [(d, (d + 1) % ways) for d in range(ways)])  43.1 us
    psum x1, blocking collectives, per_device(): lax.psum((jnp.sum(direction_q * direction_q), jnp.sum(direction_v * direc...  39.8 us
    unnamed x35, local copies, waits for them, and re-layouts  9.67 us
    dynamic_update_slice x7, local copies, waits for them, and re-layouts, gather_around(): lax.dynamic_update_slice_in_dim(full, value, (here - far) % ways * step,...  7.36 us
  transfers between devices with their start and end apart: 9, of which 8 were waited for; matrix products, arithmetic and copies ran while one was open for 7% of the time, Pallas kernels for 0%

profile of v1, /device:TPU:0, one launch (start us, length us, event | category | flops | bytes accessed | tf_op | source)
XLA Modules:
  0.0 204.8 jit_solution(6709640932893115765)
XLA Ops:
  7.2 0.0 reduce-scatter.2.cloned.1.call-start
  7.2 1.0 reshape.52
  8.2 0.8 reshape.55
  9.0 1.2 copy.40
  10.2 1.2 copy.42
  11.4 0.2 fusion.10
  11.6 0.2 fusion.7
  11.8 1.0 fusion.2
  12.8 2.3 %fusion = f32[2048,256]{0,1:T(8,128)} fusion(f32[256,2048]{1,0:T(8,128)S(1)} %fusion.2, bf16[576,2048]{1,0:T(8,128)(2,1)S(1)} %copy-done, f32[576,128]{0,1:T(8,128)S(1)} %bitcast.31, f32[576,128]{0,1:T(8,128)S(1)} %bitcast.29), kind=kOutput, calls=%fused_computation.1 | convolution fusion | flops 605241344 | bytes 7143424 | tf_op jit(solution)/shard_map/dot_general | solution.py:79
  15.2 0.0 reduce-scatter.2.cloned.1.call-update
  15.2 0.0 all-gather.2.cloned.1.call-start
  15.2 0.1 copy.39
  15.3 0.7 copy-done.7
  16.0 0.1 copy.44
  16.2 0.1 copy.46
  16.3 0.1 copy.47
  16.4 70.9 %reduce-scatter.2.cloned.1.call-done = f32[256,256]{0,1:T(8,128)} async-done(((f32[2048,256]{0,1:T(8,128)}), f32[256,256]{0,1:T(8,128)}) %reduce-scatter.2.cloned.1.call-update) | async-done | bytes 262160 | tf_op jit(solution)/shard_map/reduce_scatter | solution.py:78
  87.3 2.4 %multiply_reduce_fusion = (f32[]{:T(128)}, f32[256,128]{0,1:T(8,128)S(1)}, f32[256,128]{0,1:T(8,128)}, f32[256,128]{0,1:T(8,128)S(1)}, f32[]{:T(128)}, /*index=5...) fusion(f32[256,256]{0,1:T(8,128)} %reduce-scatter.2.cloned.1.call-done, f32[256,128]{0,1:T(8,128)S(1)} %copy.47, ...), kind=kLoop, calls=%fused_computation.14 | loop fusion | flops 720894 | bytes 1572872 | tf_op jit(solution)/shard_map/reduce_sum | solution.py:89
  89.6 39.8 %all-reduce = (f32[]{:T(128)}, f32[]{:T(128)}) all-reduce(f32[]{:T(128)} %get-tuple-element.45, f32[]{:T(128)} %get-tuple-element.37), channel_id=1, replica_groups=mesh['fs'=8,'tp'=4] {'fs','tp'}, use_global_device_ids=true, to_apply=%region_2.0 | all-reduce | flops 2 | bytes 16 | tf_op jit(solution)/shard_map/psum | solution.py:88
  130.2 1.1 convolution_multiply_fusion
  131.2 0.1 copy.52
  131.4 1.8 fusion.14
  133.9 1.1 convolution_multiply_fusion.1
  135.0 0.1 copy.51
  135.2 1.0 broadcast_in_dim.3
  136.2 1.7 constant_dynamic-update-slice_fusion.7
  137.9 2.5 %collective-permute-start = (bf16[256,256]{1,0:T(8,128)(2,1)S(1)}, bf16[256,256]{1,0:T(8,128)(2,1)S(1)}, u32[]{:S(2)}, u32[]{:S(2)}) collective-permute-start(bf16[256,256]{1,0:T(8,128)(2,1)S(1)} %get-tuple-element.35), channel_id=1, source_target_pairs={{0,4},{4,8},{8,12},{12,16},{16,20},{20,24},{24,28},{28,0},{1,5},{5... | collective-permute-start | bytes 393224 | tf_op jit(solution)/shard_map/ppermute | solution.py:19
  140.4 5.3 %collective-permute-done = bf16[256,256]{1,0:T(8,128)(2,1)S(1)} collective-permute-done((bf16[256,256]{1,0:T(8,128)(2,1)S(1)}, bf16[256,256]{1,0:T(8,128)(2,1)S(1)}, u32[]{:S(2)}, u32[]{:S(2)}) %collective-permute-start) | collective-permute-done | bytes 131104 | tf_op jit(solution)/shard_map/ppermute | solution.py:19
  145.7 1.2 collective-permute-start.1
  146.9 7.1 %collective-permute-done.1 = bf16[256,256]{1,0:T(8,128)(2,1)S(1)} collective-permute-done((bf16[256,256]{1,0:T(8,128)(2,1)S(1)}, bf16[256,256]{1,0:T(8,128)(2,1)S(1)}, u32[]{:S(2)}, u32[]{:S(2)}) %collective-permute-start.1) | collective-permute-done | bytes 131104 | tf_op jit(solution)/shard_map/ppermute | solution.py:19
  154.0 0.7 copy-done.10
  154.6 7.9 %collective-permute-done.2 = bf16[256,256]{1,0:T(8,128)(2,1)} collective-permute-done((bf16[256,256]{1,0:T(8,128)(2,1)S(1)}, bf16[256,256]{1,0:T(8,128)(2,1)}, u32[]{:S(2)}, u32[]{:S(2)}) %collective-permute-start.2) | collective-permute-done | bytes 131104 | tf_op jit(solution)/shard_map/ppermute | solution.py:19
  162.5 0.8 copy.56
  163.3 0.8 copy.55
  164.0 0.8 copy.54
  164.8 0.8 copy.53
  165.5 6.3 %collective-permute-done.3 = bf16[256,256]{1,0:T(8,128)(2,1)} collective-permute-done((bf16[256,256]{1,0:T(8,128)(2,1)}, bf16[256,256]{1,0:T(8,128)(2,1)}, u32[]{:S(2)}, u32[]{:S(2)}) %collective-permute-start.3) | collective-permute-done | bytes 131104 | tf_op jit(solution)/shard_map/ppermute | solution.py:19
  171.8 0.7 constant_dynamic-update-slice_fusion.6
  172.5 1.6 constant_dynamic-update-slice_fusion.5
  174.1 5.6 %collective-permute-done.4 = bf16[256,256]{1,0:T(8,128)(2,1)S(1)} collective-permute-done((bf16[256,256]{1,0:T(8,128)(2,1)}, bf16[256,256]{1,0:T(8,128)(2,1)S(1)}, u32[]{:S(2)}, u32[]{:S(2)}) %collective-permute-start.4) | collective-permute-done | bytes 131104 | tf_op jit(solution)/shard_map/ppermute | solution.py:19
  179.7 1.6 constant_dynamic-update-slice_fusion.4
  181.3 1.6 constant_dynamic-update-slice_fusion.3
  182.9 4.5 %collective-permute-done.5 = bf16[256,256]{1,0:T(8,128)(2,1)S(1)} collective-permute-done((bf16[256,256]{1,0:T(8,128)(2,1)S(1)}, bf16[256,256]{1,0:T(8,128)(2,1)S(1)}, u32[]{:S(2)}, u32[]{:S(2)}) %collective-permute-start.5) | collective-permute-done | bytes 131104 | tf_op jit(solution)/shard_map/ppermute | solution.py:19
  187.4 0.7 constant_dynamic-update-slice_fusion.2
  188.1 0.7 constant_dynamic-update-slice_fusion.1
  188.7 6.3 %collective-permute-done.6 = bf16[256,256]{1,0:T(8,128)(2,1)S(1)} collective-permute-done((bf16[256,256]{1,0:T(8,128)(2,1)S(1)}, bf16[256,256]{1,0:T(8,128)(2,1)S(1)}, u32[]{:S(2)}, u32[]{:S(2)}) %collective-permute-start.6) | collective-permute-done | bytes 131104 | tf_op jit(solution)/shard_map/ppermute | solution.py:19
  195.1 0.7 constant_dynamic-update-slice_fusion
  195.7 2.3 %copy.74 = bf16[2048,256]{1,0:T(8,128)(2,1)} copy(bf16[2048,256]{1,0:T(8,128)(2,1)} %all-gather.2.cloned.1.call-done) | data formatting | bytes 2097152
  (27 shorter events, 0.1 us)
Async XLA Ops:
  7.2 4.6 %copy-start = (bf16[576,2048]{1,0:T(8,128)(2,1)S(1)}, bf16[576,2048]{1,0:T(8,128)(2,1)}, u32[]{:S(2)}) copy-start(bf16[576,2048]{1,0:T(8,128)(2,1)} %param.11) | copy-start | bytes 7077892
  7.2 80.1 %reduce-scatter.2.cloned.1.call-start = ((), (), s32[]{:S(2)}) async-start(), calls=%async_computation.1 | async-start | bytes 2359296 | tf_op jit(solution)/shard_map/reduce_scatter | solution.py:78
  8.2 6.9 %copy-start.4 = (bf16[4,64,32]{1,0,2:T(4,128)(2,1)}, bf16[4,64,32]{1,0,2:T(4,128)(2,1)S(1)}, u32[]{:S(2)}) copy-start(bf16[4,64,32]{1,0,2:T(4,128)(2,1)S(1)} %reshape.52) | copy-start | bytes 49156
  9.0 6.1 %copy-start.5 = (bf16[4,64,32]{1,0,2:T(4,128)(2,1)}, bf16[4,64,32]{1,0,2:T(4,128)(2,1)S(1)}, u32[]{:S(2)}) copy-start(bf16[4,64,32]{1,0,2:T(4,128)(2,1)S(1)} %reshape.55) | copy-start | bytes 49156
  12.8 2.5 %copy-start.6 = (f32[256,128]{1,0:T(8,128)S(1)}, f32[256,128]{1,0:T(8,128)}, u32[]{:S(2)}) copy-start(f32[256,128]{1,0:T(8,128)} %param.18) | copy-start | bytes 393220
  15.1 0.9 copy-start.7
  15.1 1.0 copy-start.8
  15.1 1.1 copy-start.9
  15.2 180.5 %all-gather.2.cloned.1.call-start = ((), (), s32[]{:S(2)}) async-start(), calls=%async_computation.2 | async-start | bytes 1179648 | tf_op jit(solution)/shard_map/all_gather | solution.py:100
  131.4 32.7 %copy-start.1 = (f32[256,256]{1,0:T(8,128)}, f32[256,256]{1,0:T(8,128)S(1)}, u32[]{:S(2)}) copy-start(f32[256,256]{1,0:T(8,128)S(1)} %copy.52) | copy-start | bytes 786436
  135.1 53.6 %copy-start.2 = (f32[256,256]{1,0:T(8,128)}, f32[256,256]{1,0:T(8,128)S(1)}, u32[]{:S(2)}) copy-start(f32[256,256]{1,0:T(8,128)S(1)} %copy.51) | copy-start | bytes 786436
  135.1 27.4 %copy-start.3 = (f32[256,128]{0,1:T(8,128)S(1)}, f32[256,128]{0,1:T(8,128)}, u32[]{:S(2)}) copy-start(f32[256,128]{0,1:T(8,128)} %get-tuple-element.39) | copy-start | bytes 393220
  137.9 7.8 %collective-permute-start = (bf16[256,256]{1,0:T(8,128)(2,1)S(1)}, bf16[256,256]{1,0:T(8,128)(2,1)S(1)}, u32[]{:S(2)}, u32[]{:S(2)}) collective-permute-start(bf16[256,256]{1,0:T(8,128)(2,1)S(1)} %get-tuple-element.35), channel_id=1, source_target_pairs={{0,4},{4,8},{8,12},{12,16},{16,20},{20,24},{24,28},{28,0},{1,5},{5... | collective-permute-start | bytes 393224 | tf_op jit(solution)/shard_map/ppermute | solution.py:19
  145.7 8.3 %collective-permute-start.1 = (bf16[256,256]{1,0:T(8,128)(2,1)S(1)}, bf16[256,256]{1,0:T(8,128)(2,1)S(1)}, u32[]{:S(2)}, u32[]{:S(2)}) collective-permute-start(bf16[256,256]{1,0:T(8,128)(2,1)S(1)} %collective-permute-done), channel_id=1, source_target_pairs={{0,4},{4,8},{8,12},{12,16},{16,20},{20,24},{24,28},{28,0},{1,5},{5... | collective-permute-start | bytes 393224 | tf_op jit(solution)/shard_map/ppermute | solution.py:19
  154.0 0.7 copy-start.10
  154.6 7.9 %collective-permute-start.2 = (bf16[256,256]{1,0:T(8,128)(2,1)S(1)}, bf16[256,256]{1,0:T(8,128)(2,1)}, u32[]{:S(2)}, u32[]{:S(2)}) collective-permute-start(bf16[256,256]{1,0:T(8,128)(2,1)S(1)} %collective-permute-done.1), channel_id=1, source_target_pairs={{0,4},{4,8},{8,12},{12,16},{16,20},{20,24},{24,28},{28,0},{1,5},{5... | collective-permute-start | bytes 393224 | tf_op jit(solution)/shard_map/ppermute | solution.py:19
  162.5 9.3 %collective-permute-start.3 = (bf16[256,256]{1,0:T(8,128)(2,1)}, bf16[256,256]{1,0:T(8,128)(2,1)}, u32[]{:S(2)}, u32[]{:S(2)}) collective-permute-start(bf16[256,256]{1,0:T(8,128)(2,1)} %collective-permute-done.2), channel_id=1, source_target_pairs={{0,4},{4,8},{8,12},{12,16},{16,20},{20,24},{24,28},{28,0},{1,5},{5... | collective-permute-start | bytes 393224 | tf_op jit(solution)/shard_map/ppermute | solution.py:19
  171.8 7.9 %collective-permute-start.4 = (bf16[256,256]{1,0:T(8,128)(2,1)}, bf16[256,256]{1,0:T(8,128)(2,1)S(1)}, u32[]{:S(2)}, u32[]{:S(2)}) collective-permute-start(bf16[256,256]{1,0:T(8,128)(2,1)} %collective-permute-done.3), channel_id=1, source_target_pairs={{0,4},{4,8},{8,12},{12,16},{16,20},{20,24},{24,28},{28,0},{1,5},{5... | collective-permute-start | bytes 393224 | tf_op jit(solution)/shard_map/ppermute | solution.py:19
  179.7 7.7 %collective-permute-start.5 = (bf16[256,256]{1,0:T(8,128)(2,1)S(1)}, bf16[256,256]{1,0:T(8,128)(2,1)S(1)}, u32[]{:S(2)}, u32[]{:S(2)}) collective-permute-start(bf16[256,256]{1,0:T(8,128)(2,1)S(1)} %collective-permute-done.4), channel_id=1, source_target_pairs={{0,4},{4,8},{8,12},{12,16},{16,20},{20,24},{24,28},{28,0},{1,5},{5... | collective-permute-start | bytes 393224 | tf_op jit(solution)/shard_map/ppermute | solution.py:19
  187.4 7.7 %collective-permute-start.6 = (bf16[256,256]{1,0:T(8,128)(2,1)S(1)}, bf16[256,256]{1,0:T(8,128)(2,1)S(1)}, u32[]{:S(2)}, u32[]{:S(2)}) collective-permute-start(bf16[256,256]{1,0:T(8,128)(2,1)S(1)} %collective-permute-done.5), channel_id=1, source_target_pairs={{0,4},{4,8},{8,12},{12,16},{16,20},{20,24},{24,28},{28,0},{1,5},{5... | collective-permute-start | bytes 393224 | tf_op jit(solution)/shard_map/ppermute | solution.py:19
Sparse Core Ops, SparseCore 0:
  15.3 71.9 reduce-scatter.1
  133.4 42.8 all-gather.1
